TPU v7x, 32 devices: a whole 2x2x4 slice. The times are simulated.
32 devices in a mesh: sp: 8 (over z, x), tp: 4 (over y, core).
Axes of the slice: x: 2, y: 2, z: 4, core: 2. Of those that a mesh axis runs over, the one named last changes fastest.
Arguments:
- residual_in: bfloat16 [8192, 2048], P(('sp', 'tp')), may hold values from -6 to 6
- gate_outer: bfloat16 [8192, 1024], P('sp', 'tp'), may hold values from -6 to 6
- gate_inner: bfloat16 [8192, 1024], P('sp', 'tp'), may hold values from -6 to 6
- conv_input: bfloat16 [8192, 1024], P('sp', 'tp'), may hold values from -6 to 6
- conv_taps: bfloat16 [3, 1024], P(None, 'tp'), may hold values from -5 to 5
- norm_gain: bfloat16 [1024], P('tp'), may hold values from 0.099609375 to 1.8984375
- out_weight: bfloat16 [1024, 2048], P('tp'), may hold values from -0.1875 to 0.1875
- moe_gain: bfloat16 [2048], replicated, may hold values from 0.099609375 to 1.8984375
- expert_ids: int32 [8192, 2], P(('sp', 'tp')), may hold values from 0 to 7, all different within a row; in each aligned block of 256 rows (0 to 255, 256 to 511, ...) at most 128 rows name the same one
- group_prob: float32 [8192], P(('sp', 'tp')), may hold values from 0.3 to 1
- route_prob: float32 [8192, 2], P(('sp', 'tp')), may hold values from 0.1 to 1
- expert_gate: bfloat16 [8, 2048, 512], P('sp'), may hold values from -0.125 to 0.125
- expert_up: bfloat16 [8, 2048, 512], P('sp'), may hold values from -0.125 to 0.125
- expert_down: bfloat16 [8, 512, 2048], P('sp'), may hold values from -0.25 to 0.25
Outputs:
- layer_out: bfloat16 [8192, 2048], P(('sp', 'tp'))
Inputs may be any that keep to these rules, and one draw needn't show every extreme that they name: `expert_ids`: each row names 2 different experts. Within the rows of one device (aligned blocks of 256 rows) no expert is named more than 128 times.
All inputs are finite; a program needn't handle non-finite values.
Results may differ from a plain program's by a relative error of at most 0.0075.
Values may be sent and summed in bfloat16 or wider, within the bound.
A program may use at most 64 MiB of HBM per device.

v0:
```python
import jax
import jax.numpy as jnp
from jax import lax
from jax.experimental import pallas as pl
from jax.experimental.pallas import tpu as pltpu
from jax.sharding import PartitionSpec as P

MESH = pl.DeviceIdType.MESH
EPSILON = 1e-06


def from_behind(shard, axis, by):
    devices = lax.axis_size(axis)
    pairs = [(i, i + by) for i in range(devices) if 0 <= i + by < devices]
    return lax.ppermute(shard, axis, pairs)


def rms_norm(values, gain):
    floats = values.astype(jnp.float32)
    factor = lax.rsqrt(jnp.mean(floats * floats, axis=-1, keepdims=True) + EPSILON)
    return floats * factor * gain.astype(jnp.float32)


GATHER_BYTES = 26 * 2**20
GAIN_ROWS = 16
HALO_ROWS = 16
PARTS = 4
COPIES = 64


def layer_kernel(
    outer_ref, inner_ref, input_ref, taps_ref, gain_ref, weight_ref, residual_ref, moe_ref, ids_ref, group_ref, route_ref,
    gate_hbm, up_hbm, down_hbm,
    out_ref,
    halo, sent, got, weights, both, down, tokens, near, far, near_line, far_in, far_line, columns,
    residual_sc, own_acc, line_out, line_in, pair_out, pair_in, hold, back_out, back_in, hidden_sc,
    send_sem, recv_sem, local_sem,
):
    sp, tp = lax.axis_index("sp"), lax.axis_index("tp")
    sp_size, tp_size = lax.axis_size("sp"), lax.axis_size("tp")
    core_me, line_me = tp % 2, (tp // 2) % 2
    core_bit = 1 - 2 * core_me
    line_bit = 2 - 4 * line_me
    lanes = [tp, tp + core_bit, tp + line_bit, tp + line_bit + core_bit]
    core, line = (sp, lanes[1]), (sp, lanes[2])
    x_peer = (sp + 1 - 2 * (sp % 2), tp)
    z_peer = (sp + 2 - 4 * ((sp // 2) % 2), tp)
    cross = ((sp + sp_size // 2) % sp_size, tp)
    after, before = ((sp + 1) % sp_size, tp), ((sp + sp_size - 1) % sp_size, tp)
    peers = [core, line, (sp, lanes[3]), x_peer, z_peer, cross, after, before]

    units = down.shape[2]
    slots, cuts = down.shape[0], down.shape[1]
    fetched = []
    for cut in range(cuts):
        first = pl.multiple_of((line_me * cuts + cut) * units, units)
        fetched += [
            pltpu.make_async_copy(gate_hbm.at[0, :, pl.ds(first, units)], both.at[0, cut, :, pl.ds(0, units)], local_sem.at[3 * cut]),
            pltpu.make_async_copy(up_hbm.at[0, :, pl.ds(first, units)], both.at[0, cut, :, pl.ds(units, units)], local_sem.at[3 * cut + 1]),
            pltpu.make_async_copy(down_hbm.at[0, pl.ds(first, units), :], down.at[0, cut], local_sem.at[3 * cut + 2]),
        ]
    for copy in fetched:
        copy.start()

    barrier = pltpu.get_barrier_semaphore()
    for peer in peers:
        pl.semaphore_signal(barrier, inc=1, device_id=peer, device_id_type=MESH)
    pl.semaphore_wait(barrier, len(peers))

    started = []

    def send(source, target, peer):
        number = len(started)
        copy = pltpu.make_async_remote_copy(
            src_ref=source, dst_ref=target, send_sem=send_sem.at[number], recv_sem=recv_sem.at[number],
            device_id=peer, device_id_type=MESH,
        )
        copy.start()
        started.append(copy)
        return copy

    full = inner_ref.shape[0]
    halos = [
        send(inner_ref.at[pl.ds(full - HALO_ROWS, HALO_ROWS)], halo.at[0], after),
        send(input_ref.at[pl.ds(full - HALO_ROWS, HALO_ROWS)], halo.at[1], after),
    ]
    weight_line = send(weight_ref, weights.at[1], line)
    weight_core = send(weight_ref, weights.at[0], core)
    for copy in fetched:
        copy.wait()
    x_both = send(both.at[0, core_me], both.at[1, core_me], x_peer)
    z_both = send(both.at[0, core_me], both.at[2, core_me], z_peer)
    x_down = send(down.at[0, core_me], down.at[1, core_me], x_peer)
    z_down = send(down.at[0, core_me], down.at[2, core_me], z_peer)

    ids = ids_ref[...]
    route = route_ref[...]
    scale = group_ref[...] * route / jnp.sum(route, axis=0, keepdims=True)
    half = sp_size // 2
    for slot in range(slots):
        side = (sp % half) ^ slot
        for table, base in ((near, (sp // half) * half), (far, (1 - sp // half) * half)):
            chosen = jnp.where(ids == base + side, scale, 0.0)
            table[slot : slot + 1, :] = jnp.sum(chosen, axis=0, keepdims=True)

    for copy in halos:
        copy.wait_recv()
    rows, width = residual_ref.shape
    taps = taps_ref[...].astype(jnp.float32)
    count = taps.shape[0]
    exchanged = []
    for step in (2, 3, 1, 0):
        block = lanes[step]
        first = pl.multiple_of(block * rows, rows)
        inner = inner_ref[pl.ds(first, rows)].astype(jnp.float32) * input_ref[pl.ds(first, rows)].astype(jnp.float32)
        back = pl.multiple_of(jnp.maximum(block * rows - HALO_ROWS, 0), HALO_ROWS)
        behind = inner_ref[pl.ds(back, HALO_ROWS)].astype(jnp.float32) * input_ref[pl.ds(back, HALO_ROWS)].astype(jnp.float32)
        outside = halo[0].astype(jnp.float32) * halo[1].astype(jnp.float32)
        outside = jnp.where(sp == 0, 0.0, outside)
        behind = jnp.where(block == 0, outside, behind)
        padded = jnp.concatenate([behind, inner], axis=0)
        filtered = jnp.zeros_like(inner)
        for offset in range(count):
            start = HALO_ROWS - (count - 1) + offset
            filtered = filtered + taps[offset][None, :] * padded[start : start + rows]
        mixed = (outer_ref[pl.ds(first, rows)].astype(jnp.float32) * filtered).astype(jnp.bfloat16)
        sent[step, :rows] = mixed
        sent[step, rows:] = jnp.broadcast_to(gain_ref[...], (GAIN_ROWS, mixed.shape[1]))
        if step > 0:
            exchanged.append(send(sent.at[step], got.at[step - 1], (sp, block)))
    near_copy = send(near, near_line, line)
    far_copy = send(far, far_in, cross)

    for copy in exchanged:
        copy.wait_recv()
    blocks = [sent.at[0], got.at[0], got.at[1], got.at[2]]
    total = jnp.zeros((rows, 1), jnp.float32)
    for block in blocks:
        values = block[:rows].astype(jnp.float32)
        total = total + jnp.sum(values * values, axis=1, keepdims=True)
    factor = lax.rsqrt(total / (tp_size * inner_ref.shape[1]) + EPSILON)

    def normed(block):
        gain = block[rows:][:1].astype(jnp.float32)
        return (block[:rows].astype(jnp.float32) * factor * gain).astype(jnp.bfloat16)

    weight_line.wait_recv()
    weight_both = send(weights.at[1], weights.at[2], core)
    weight_core.wait_recv()
    out = residual_ref[...].astype(jnp.float32)
    out = out + jnp.dot(normed(blocks[0]), weight_ref[...], preferred_element_type=jnp.float32)
    out = out + jnp.dot(normed(blocks[1]), weights[0], preferred_element_type=jnp.float32)
    out = out + jnp.dot(normed(blocks[2]), weights[1], preferred_element_type=jnp.float32)
    weight_both.wait_recv()
    out = out + jnp.dot(normed(blocks[3]), weights[2], preferred_element_type=jnp.float32)
    residual = out.astype(jnp.bfloat16)
    residual_sc[...] = residual
    floats = residual.astype(jnp.float32)
    mean = jnp.mean(floats * floats, axis=1, keepdims=True)
    routed = (floats * lax.rsqrt(mean + EPSILON) * moe_ref[...].astype(jnp.float32)).astype(jnp.bfloat16)

    piece = rows // PARTS
    batch = 2 * piece
    own_at, line_at, pair_at = (4, 5), (2, 3), (0, 1, 6, 7)
    for number, unit in enumerate(own_at):
        tokens[unit] = routed[number * batch : (number + 1) * batch]

    def own_rows(part):
        return tokens.at[own_at[part // 2], pl.ds((part % 2) * piece, piece)]

    def line_rows(part):
        return tokens.at[line_at[part // 2], pl.ds((part % 2) * piece, piece)]

    across, shared, beside = [], [], []

    def send_across(part):
        across.append(send(own_rows(part), tokens.at[pair_at[part], pl.ds(0, piece)], cross))

    def send_shared(part):
        shared.append(send(own_rows(part), line_rows(part), line))

    def relay(part):
        across[part].wait_recv()
        here = tokens.at[pair_at[part], pl.ds(0, piece)]
        beside.append(send(here, tokens.at[pair_at[part], pl.ds(piece, piece)], line))

    for part in range(PARTS):
        send_across(part)
    send_shared(0)
    send_shared(1)

    far_copy.wait_recv()
    far_relay = send(far_in, far_line, line)
    near_copy.wait_recv()

    def across_core(slot):
        return [
            send(both.at[slot, core_me], both.at[slot, core_me], core),
            send(down.at[slot, core_me], down.at[slot, core_me], core),
        ]

    x_both.wait_recv()
    x_down.wait_recv()
    diagonal_down = send(down.at[1, core_me], down.at[3, core_me], z_peer)
    z_both.wait_recv()
    diagonal_both = send(both.at[2, core_me], both.at[3, core_me], x_peer)
    z_down.wait_recv()
    cores = across_core(1) + across_core(2)

    relay(0)
    send_shared(2)
    far_relay.wait_recv()
    for slot in range(slots):
        for unit, table in ((own_at, near), (line_at, near_line)):
            column = table[slot : slot + 1, :].T
            for number in range(2):
                columns[slot, unit[number]] = column[number * batch : (number + 1) * batch]
        here, there = far_in[slot : slot + 1, :].T, far_line[slot : slot + 1, :].T
        for part in range(PARTS):
            take = slice(part * piece, (part + 1) * piece)
            columns[slot, pair_at[part], :piece] = here[take]
            columns[slot, pair_at[part], piece:] = there[take]
    relay(1)
    send_shared(3)
    diagonal_both.wait_recv()
    diagonal_down.wait_recv()
    cores += across_core(3)
    for copy in cores:
        copy.wait_recv()

    def expert_sum(unit, store):
        rows_in = tokens[unit]
        for slot in range(slots):
            scale_in = columns[slot, unit]
            for cut in range(cuts):
                act = jnp.dot(rows_in, both[slot, cut], preferred_element_type=jnp.float32)
                gated = jax.nn.silu(act[:, :units]) * act[:, units:]
                start = (slot * cuts + cut) * units
                hidden_sc[:, start : start + units] = (scale_in * gated).astype(jnp.bfloat16)
        hidden = hidden_sc[...]
        step = width // 4
        for tile in range(4):
            columns_at = pl.ds(tile * step, step)
            matrix = down[:, :, :, tile * step : (tile + 1) * step].reshape(slots * cuts * units, step)
            store(columns_at, jnp.dot(hidden, matrix, preferred_element_type=jnp.float32))

    pairs, lines, returned = [], [], []

    def pair_step(part):
        beside[part].wait_recv()

        def store(columns_at, value):
            hold[part, :, columns_at] = value[:piece]
            pair_out[part, :, columns_at] = value[piece:].astype(jnp.bfloat16)

        expert_sum(pair_at[part], store)
        pairs.append(send(pair_out.at[part], pair_in.at[part], line))

    def return_step(part):
        pairs[part].wait_recv()
        back_out[part] = (hold[part] + pair_in[part].astype(jnp.float32)).astype(jnp.bfloat16)
        returned.append(send(back_out.at[part], back_in.at[part], cross))

    def line_step(number):
        for part in (2 * number, 2 * number + 1):
            shared[part].wait_recv()

        def store(columns_at, value):
            line_out[number, :, columns_at] = value.astype(jnp.bfloat16)

        expert_sum(line_at[number], store)
        lines.append(send(line_out.at[number], line_in.at[number], line))

    def own_step(number):
        def store(columns_at, value):
            own_acc[number, :, columns_at] = value

        expert_sum(own_at[number], store)

    pair_step(0)
    pair_step(1)
    relay(2)
    return_step(0)
    line_step(0)
    return_step(1)
    line_step(1)
    relay(3)
    pair_step(2)
    own_step(0)
    pair_step(3)
    return_step(2)
    own_step(1)
    return_step(3)
    for number in range(2):
        lines[number].wait_recv()
        take = pl.ds(number * batch, batch)
        own_acc[number] += residual_sc[take].astype(jnp.float32) + line_in[number].astype(jnp.float32)
    for part in range(PARTS):
        returned[part].wait_recv()
        inside = pl.ds((part % 2) * piece, piece)
        value = own_acc[part // 2, inside] + back_in[part].astype(jnp.float32)
        out_ref[pl.ds(part * piece, piece)] = value.astype(jnp.bfloat16)
    for copy in started:
        copy.wait_send()


def half_slice(
    residual_in,
    gate_outer,
    gate_inner,
    conv_input,
    conv_taps,
    norm_gain,
    out_weight,
    moe_gain,
    expert_ids,
    group_prob,
    route_prob,
    expert_gate,
    expert_up,
    expert_down,
):
    sp, tp = lax.axis_size("sp"), lax.axis_size("tp")
    rows, width = residual_in.shape
    channels = gate_outer.shape[1]
    slots, cuts = sp // 2, 2
    units = expert_gate.shape[2] // tp
    piece = rows // PARTS
    wide = slots * cuts * units
    vmem = pl.BlockSpec(memory_space=pltpu.VMEM)
    hbm = pl.BlockSpec(memory_space=pl.ANY)
    half = lambda *shape: pltpu.VMEM(shape, jnp.bfloat16)
    single = lambda *shape: pltpu.VMEM(shape, jnp.float32)
    return pl.pallas_call(
        layer_kernel,
        in_specs=[vmem] * 11 + [hbm] * 3,
        out_specs=vmem,
        out_shape=jax.ShapeDtypeStruct((rows, width), jnp.bfloat16),
        scratch_shapes=[
            half(2, HALO_ROWS, channels),
            half(tp, rows + GAIN_ROWS, channels),
            half(tp - 1, rows + GAIN_ROWS, channels),
            half(tp - 1, *out_weight.shape),
            half(slots, cuts, width, 2 * units),
            half(slots, cuts, units, width),
            half(8, 2 * piece, width),
            single(slots, rows),
            single(slots, rows),
            single(slots, rows),
            single(slots, rows),
            single(slots, rows),
            single(slots, 8, 2 * piece, 1),
            half(rows, width),
            single(2, 2 * piece, width),
            half(2, 2 * piece, width),
            half(2, 2 * piece, width),
            half(PARTS, piece, width),
            half(PARTS, piece, width),
            single(PARTS, piece, width),
            half(PARTS, piece, width),
            half(PARTS, piece, width),
            half(2 * piece, wide),
            pltpu.SemaphoreType.DMA((COPIES,)),
            pltpu.SemaphoreType.DMA((COPIES,)),
            pltpu.SemaphoreType.DMA((6,)),
        ],
        compiler_params=pltpu.CompilerParams(
            collective_id=0, has_side_effects=True, vmem_limit_bytes=56 * 2**20
        ),
    )(
        gate_outer, gate_inner, conv_input, conv_taps, norm_gain[None], out_weight, residual_in, moe_gain[None],
        expert_ids.T, group_prob[None], route_prob.T, expert_gate, expert_up, expert_down,
    )


def exchange_slots(
    residual_in,
    gate_outer,
    gate_inner,
    conv_input,
    conv_taps,
    norm_gain,
    out_weight,
    moe_gain,
    expert_ids,
    group_prob,
    route_prob,
    expert_gate,
    expert_up,
    expert_down,
):
    seq_rows, channels = conv_input.shape
    taps_count = conv_taps.shape[0]
    inner = gate_inner.astype(jnp.float32) * conv_input.astype(jnp.float32)
    earlier = from_behind(inner[seq_rows - (taps_count - 1) :], "sp", 1)
    padded = jnp.concatenate([earlier, inner], axis=0)
    tap_f = conv_taps.astype(jnp.float32)
    filtered = jnp.zeros((seq_rows, channels), jnp.float32)
    for offset in range(taps_count):
        filtered = filtered + tap_f[offset][None, :] * padded[offset : offset + seq_rows]
    mixed_out = (gate_outer.astype(jnp.float32) * filtered).astype(jnp.bfloat16)
    gathered = lax.all_to_all(mixed_out, "tp", split_axis=0, concat_axis=1, tiled=True)
    full_weight, full_gain = (
        lax.all_gather(out_weight, "tp", axis=0, tiled=True),
        lax.all_gather(norm_gain, "tp", axis=0, tiled=True),
    )
    normed = rms_norm(gathered, full_gain).astype(jnp.bfloat16)
    projected = jnp.dot(normed, full_weight, preferred_element_type=jnp.float32)
    residual = (residual_in.astype(jnp.float32) + projected).astype(jnp.bfloat16)
    routed_in = rms_norm(residual, moe_gain).astype(jnp.bfloat16)
    tok_rows, width = routed_in.shape
    top_count = expert_ids.shape[1]
    local_count = expert_gate.shape[0]
    group_count = lax.axis_size("sp")
    experts_all = local_count * group_count
    capacity = 2 * tok_rows * top_count // experts_all
    slots = tok_rows * top_count
    flat_e = expert_ids.reshape(-1)
    one_hot = (flat_e[:, None] == jnp.arange(experts_all, dtype=jnp.int32)[None, :]).astype(
        jnp.int32
    )
    slot_rank = jnp.sum((jnp.cumsum(one_hot, axis=0) - 1) * one_hot, axis=1)
    owner_dev = flat_e // local_count
    local_slot = flat_e % local_count
    position = (local_slot * group_count + owner_dev) * capacity + slot_rank
    source_slot = (
        jnp.full((experts_all * capacity,), slots, jnp.int32)
        .at[position]
        .set(jnp.arange(slots, dtype=jnp.int32))
    )
    rows_pad = jnp.concatenate([routed_in, jnp.zeros((1, width), jnp.bfloat16)], axis=0)
    outgoing = rows_pad[source_slot // top_count].reshape(local_count, group_count, capacity, width)
    arrived = lax.all_to_all(outgoing, "sp", split_axis=1, concat_axis=1, tiled=True)
    gate_act = jnp.einsum(
        "esrd,edf->esrf", arrived, expert_gate, preferred_element_type=jnp.float32
    )
    up_act = jnp.einsum("esrd,edf->esrf", arrived, expert_up, preferred_element_type=jnp.float32)
    hidden = (jax.nn.silu(gate_act) * up_act).astype(jnp.bfloat16)
    result = jnp.einsum(
        "esrf,efd->esrd", hidden, expert_down, preferred_element_type=jnp.float32
    ).astype(jnp.bfloat16)
    returned = lax.all_to_all(result, "sp", split_axis=1, concat_axis=1, tiled=True)
    slot_out = returned.reshape(-1, width)[position].reshape(tok_rows, top_count, width)
    weights = group_prob[:, None] * route_prob / jnp.sum(route_prob, axis=1, keepdims=True)
    expert_sum = jnp.sum(slot_out.astype(jnp.float32) * weights[:, :, None], axis=1)
    return (residual.astype(jnp.float32) + expert_sum).astype(jnp.bfloat16)


def solution(mesh):
    in_specs = (
        P(("sp", "tp"), None),
        P("sp", "tp"),
        P("sp", "tp"),
        P("sp", "tp"),
        P(None, "tp"),
        P("tp"),
        P("tp", None),
        P(),
        P(("sp", "tp"), None),
        P(("sp", "tp")),
        P(("sp", "tp"), None),
        P("sp", None, None),
        P("sp", None, None),
        P("sp", None, None),
    )
    out_specs = P(("sp", "tp"), None)
    sp, tp = mesh.shape["sp"], mesh.shape["tp"]

    def body(*args):
        gate, outer = args[11], args[1]
        gathered = 3 * gate.size * gate.dtype.itemsize * sp // 4
        pairs = gate.shape[0] == 1 and sp == 8 and tp == 4
        sized = gate.shape[2] == 128 * tp and outer.shape[0] % (256 * tp) == 0
        if pairs and sized and gathered <= GATHER_BYTES:
            return half_slice(*args)
        return exchange_slots(*args)

    return jax.shard_map(body, mesh=mesh, in_specs=in_specs, out_specs=out_specs, check_vma=False)
```

profile of v0, /device:TPU:0, one launch (start us, length us, event | category | flops | bytes accessed | tf_op | source)
XLA Modules:
  0.0 166.1 jit_solution(17276195919396872111)
XLA Ops:
  0.0 1.2 broadcast_in_dim.9.gain_ref
  1.2 1.3 broadcast_in_dim.10.moe_ref
  2.5 161.2 %shard_map.136 = bf16[256,2048]{1,0:T(8,128)(2,1)} custom-call(bf16[1024,256]{1,0:T(8,128)(2,1)} %outer_ref.1, bf16[1024,256]{1,0:T(8,128)(2,1)} %inner_ref.1, bf16[1024,256]{1,0:T(8,128)(2,1)} %input_ref.1, bf16[3,256]{1,0:T(4,128)(2,1)} %taps_ref.1, bf16[1,256]{1,0:T(2,128)(2,1)} %broadcast_in_dim.9.gain_ref, bf16[256,2048]{1,0:T(8,128)(2,1)} %weight_ref.1, ...), custom_call_target="tpu_custom_call" | custom-call | tf_op jit(solution)/shard_map/pallas_call | solution.py:334
  163.8 2.3 %copy.16 = bf16[256,2048]{1,0:T(8,128)(2,1)} copy(bf16[256,2048]{1,0:T(8,128)(2,1)} %shard_map.136) | data formatting | bytes 2097152
where the time goes:
time: 166 us
  Pallas kernels  161 us (97%)
  local copies, waits for them, and re-layouts  4.84 us (3%)
    pallas_call x1, Pallas kernels, half_slice(): pl.pallas_call(layer_kernel, in_specs=[vmem] * 11 + [hbm] * 3, out_specs=...  161 us

commit v1 on v0

--- a/solution.py
+++ b/solution.py
@@ -29,9 +29,10 @@
 
 
 def layer_kernel(
-    outer_ref, inner_ref, input_ref, taps_ref, gain_ref, weight_ref, residual_ref, moe_ref, ids_ref, group_ref, route_ref,
-    gate_hbm, up_hbm, down_hbm,
+    outer_hbm, inner_hbm, input_hbm, taps_hbm, weight_hbm, residual_hbm, ids_hbm, group_hbm, route_hbm,
+    gate_hbm, up_hbm, down_hbm, gain_ref, moe_ref,
     out_ref,
+    outer_ref, inner_ref, input_ref, taps_ref, weight_ref, residual_ref, ids_ref, group_ref, route_ref,
     halo, sent, got, weights, both, down, tokens, near, far, near_line, far_in, far_line, columns,
     residual_sc, own_acc, line_out, line_in, pair_out, pair_in, hold, back_out, back_in, hidden_sc,
     send_sem, recv_sem, local_sem,
@@ -49,6 +50,15 @@
     after, before = ((sp + 1) % sp_size, tp), ((sp + sp_size - 1) % sp_size, tp)
     peers = [core, line, (sp, lanes[3]), x_peer, z_peer, cross, after, before]
 
+    loaded = {}
+    for number, (name, source, target) in enumerate((
+        ("weight", weight_hbm, weight_ref), ("inner", inner_hbm, inner_ref), ("input", input_hbm, input_ref),
+        ("outer", outer_hbm, outer_ref), ("taps", taps_hbm, taps_ref), ("ids", ids_hbm, ids_ref),
+        ("group", group_hbm, group_ref), ("route", route_hbm, route_ref), ("residual", residual_hbm, residual_ref),
+    )):
+        loaded[name] = pltpu.make_async_copy(source, target, local_sem.at[6 + number])
+        loaded[name].start()
+
     units = down.shape[2]
     slots, cuts = down.shape[0], down.shape[1]
     fetched = []
@@ -69,30 +79,53 @@
 
     started = []
 
-    def send(source, target, peer):
+    def prepare(source, target, peer):
         number = len(started)
         copy = pltpu.make_async_remote_copy(
             src_ref=source, dst_ref=target, send_sem=send_sem.at[number], recv_sem=recv_sem.at[number],
             device_id=peer, device_id_type=MESH,
         )
-        copy.start()
         started.append(copy)
         return copy
 
+    def send(source, target, peer):
+        copy = prepare(source, target, peer)
+        copy.start()
+        return copy
+
+    for name in ("weight", "inner", "input"):
+        loaded[name].wait()
     full = inner_ref.shape[0]
+    rows, width = residual_ref.shape
+    ends = (sp < 2) | (sp >= sp_size - 2)
+    middle = jnp.logical_not(ends)
     halos = [
         send(inner_ref.at[pl.ds(full - HALO_ROWS, HALO_ROWS)], halo.at[0], after),
         send(input_ref.at[pl.ds(full - HALO_ROWS, HALO_ROWS)], halo.at[1], after),
     ]
-    weight_line = send(weight_ref, weights.at[1], line)
+    quarter = weight_ref.shape[0] // 4
+    x_me = sp % 2
+
+    def weight_rows(side, number):
+        return pl.ds(pl.multiple_of((2 * side + number) * quarter, quarter), quarter)
+
+    weight_line = [
+        send(weight_ref.at[weight_rows(x_me, number)], weights.at[1, weight_rows(x_me, number)], line) for number in range(2)
+    ]
     weight_core = send(weight_ref, weights.at[0], core)
     for copy in fetched:
         copy.wait()
-    x_both = send(both.at[0, core_me], both.at[1, core_me], x_peer)
+    unit_half = units // 2
+
+    def down_rows(slot, number):
+        return down.at[slot, core_me, pl.ds(number * unit_half, unit_half)]
+
+    x_down = [send(down_rows(0, 0), down_rows(1, 0), x_peer)]
     z_both = send(both.at[0, core_me], both.at[2, core_me], z_peer)
-    x_down = send(down.at[0, core_me], down.at[1, core_me], x_peer)
     z_down = send(down.at[0, core_me], down.at[2, core_me], z_peer)
 
+    for name in ("ids", "group", "route", "outer", "taps", "residual"):
+        loaded[name].wait()
     ids = ids_ref[...]
     route = route_ref[...]
     scale = group_ref[...] * route / jnp.sum(route, axis=0, keepdims=True)
@@ -105,7 +138,6 @@
 
     for copy in halos:
         copy.wait_recv()
-    rows, width = residual_ref.shape
     taps = taps_ref[...].astype(jnp.float32)
     count = taps.shape[0]
     exchanged = []
@@ -125,45 +157,67 @@
             filtered = filtered + taps[offset][None, :] * padded[start : start + rows]
         mixed = (outer_ref[pl.ds(first, rows)].astype(jnp.float32) * filtered).astype(jnp.bfloat16)
         sent[step, :rows] = mixed
-        sent[step, rows:] = jnp.broadcast_to(gain_ref[...], (GAIN_ROWS, mixed.shape[1]))
+        sent[step, rows:] = jnp.broadcast_to(gain_ref[...].reshape(1, -1), (GAIN_ROWS, mixed.shape[1]))
         if step > 0:
             exchanged.append(send(sent.at[step], got.at[step - 1], (sp, block)))
     near_copy = send(near, near_line, line)
     far_copy = send(far, far_in, cross)
 
-    for copy in exchanged:
-        copy.wait_recv()
-    blocks = [sent.at[0], got.at[0], got.at[1], got.at[2]]
-    total = jnp.zeros((rows, 1), jnp.float32)
-    for block in blocks:
-        values = block[:rows].astype(jnp.float32)
-        total = total + jnp.sum(values * values, axis=1, keepdims=True)
-    factor = lax.rsqrt(total / (tp_size * inner_ref.shape[1]) + EPSILON)
-
-    def normed(block):
-        gain = block[rows:][:1].astype(jnp.float32)
-        return (block[:rows].astype(jnp.float32) * factor * gain).astype(jnp.bfloat16)
-
-    weight_line.wait_recv()
-    weight_both = send(weights.at[1], weights.at[2], core)
-    weight_core.wait_recv()
-    out = residual_ref[...].astype(jnp.float32)
-    out = out + jnp.dot(normed(blocks[0]), weight_ref[...], preferred_element_type=jnp.float32)
-    out = out + jnp.dot(normed(blocks[1]), weights[0], preferred_element_type=jnp.float32)
-    out = out + jnp.dot(normed(blocks[2]), weights[1], preferred_element_type=jnp.float32)
-    weight_both.wait_recv()
-    out = out + jnp.dot(normed(blocks[3]), weights[2], preferred_element_type=jnp.float32)
-    residual = out.astype(jnp.bfloat16)
-    residual_sc[...] = residual
-    floats = residual.astype(jnp.float32)
-    mean = jnp.mean(floats * floats, axis=1, keepdims=True)
-    routed = (floats * lax.rsqrt(mean + EPSILON) * moe_ref[...].astype(jnp.float32)).astype(jnp.bfloat16)
-
     piece = rows // PARTS
     batch = 2 * piece
+    blocks = [sent.at[0], got.at[0], got.at[1], got.at[2]]
+    matrices = [weight_ref, weights.at[0], weights.at[1], weights.at[2]]
+
+    def gained(block, take):
+        gain = block[rows:][:1].astype(jnp.float32)
+        return (block[take].astype(jnp.float32) * gain).astype(jnp.bfloat16)
+
+    def squares(block):
+        values = block[:rows].astype(jnp.float32)
+        return jnp.sum(values * values, axis=1, keepdims=True)
+
+    def product(number, take):
+        return jnp.dot(gained(blocks[number], take), matrices[number][...], preferred_element_type=jnp.float32)
+
+    exchanged[2].wait_recv()
+    weight_core.wait_recv()
+    for number in range(2):
+        take = slice(number * batch, (number + 1) * batch)
+        own_acc[number] = product(0, take) + product(1, take)
+    partial = squares(blocks[0]) + squares(blocks[1])
+
+    weight_x, weight_both = [], []
+    for number in range(2):
+        weight_line[number].wait_recv()
+        arrived = weights.at[1, weight_rows(x_me, number)]
+        weight_x.append(send(arrived, arrived, x_peer))
+        weight_both.append(send(arrived, weights.at[2, weight_rows(x_me, number)], core))
+    x_down.append(send(down_rows(0, 1), down_rows(1, 1), x_peer))
+    x_both = send(both.at[0, core_me], both.at[1, core_me], x_peer)
+    x_down[0].wait_recv()
+    diagonal_down = [send(down_rows(1, 0), down_rows(3, 0), z_peer)]
+    for number in range(2):
+        weight_x[number].wait_recv()
+        arrived = weights.at[1, weight_rows(1 - x_me, number)]
+        weight_both.append(send(arrived, weights.at[2, weight_rows(1 - x_me, number)], core))
+
+    for copy in exchanged[:2]:
+        copy.wait_recv()
+    total = partial + squares(blocks[2]) + squares(blocks[3])
+    factor = lax.rsqrt(total / (tp_size * inner_ref.shape[1]) + EPSILON)
+    for copy in weight_both:
+        copy.wait_recv()
     own_at, line_at, pair_at = (4, 5), (2, 3), (0, 1, 6, 7)
     for number, unit in enumerate(own_at):
-        tokens[unit] = routed[number * batch : (number + 1) * batch]
+        take = slice(number * batch, (number + 1) * batch)
+        projected = own_acc[number] + product(2, take) + product(3, take)
+        out = residual_ref[take].astype(jnp.float32) + factor[take] * projected
+        residual = out.astype(jnp.bfloat16)
+        residual_sc[take] = residual
+        floats = residual.astype(jnp.float32)
+        mean = jnp.mean(floats * floats, axis=1, keepdims=True)
+        routed = floats * lax.rsqrt(mean + EPSILON) * moe_ref[...].reshape(1, -1).astype(jnp.float32)
+        tokens[unit] = routed.astype(jnp.bfloat16)
 
     def own_rows(part):
         return tokens.at[own_at[part // 2], pl.ds((part % 2) * piece, piece)]
@@ -171,44 +225,42 @@
     def line_rows(part):
         return tokens.at[line_at[part // 2], pl.ds((part % 2) * piece, piece)]
 
-    across, shared, beside = [], [], []
-
-    def send_across(part):
-        across.append(send(own_rows(part), tokens.at[pair_at[part], pl.ds(0, piece)], cross))
-
-    def send_shared(part):
-        shared.append(send(own_rows(part), line_rows(part), line))
-
-    def relay(part):
-        across[part].wait_recv()
-        here = tokens.at[pair_at[part], pl.ds(0, piece)]
-        beside.append(send(here, tokens.at[pair_at[part], pl.ds(piece, piece)], line))
-
-    for part in range(PARTS):
-        send_across(part)
-    send_shared(0)
-    send_shared(1)
+    def pair_rows(part, second):
+        return tokens.at[pair_at[part], pl.ds(second * piece, piece)]
+
+    across = [send(own_rows(part), pair_rows(part, 0), cross) for part in range(PARTS)]
+    shared = [prepare(own_rows(part), line_rows(part), line) for part in range(PARTS)]
+    beside = [prepare(pair_rows(part, 0), pair_rows(part, 1), line) for part in range(PARTS)]
+    for copy in shared:
+        copy.start()
+
+    def relay(parts):
+        for part in parts:
+            across[part].wait_recv()
+            beside[part].start()
 
     far_copy.wait_recv()
     far_relay = send(far_in, far_line, line)
     near_copy.wait_recv()
 
-    def across_core(slot):
-        return [
-            send(both.at[slot, core_me], both.at[slot, core_me], core),
-            send(down.at[slot, core_me], down.at[slot, core_me], core),
-        ]
-
-    x_both.wait_recv()
-    x_down.wait_recv()
-    diagonal_down = send(down.at[1, core_me], down.at[3, core_me], z_peer)
     z_both.wait_recv()
     diagonal_both = send(both.at[2, core_me], both.at[3, core_me], x_peer)
+    cores = [send(both.at[2, core_me], both.at[2, core_me], core)]
+    x_down[1].wait_recv()
+    diagonal_down.append(send(down_rows(1, 1), down_rows(3, 1), z_peer))
+    cores.append(send(down.at[1, core_me], down.at[1, core_me], core))
+
+    @pl.when(middle)
+    def _():
+        relay((0, 1))
+
     z_down.wait_recv()
-    cores = across_core(1) + across_core(2)
-
-    relay(0)
-    send_shared(2)
+    cores.append(send(down.at[2, core_me], down.at[2, core_me], core))
+
+    @pl.when(middle)
+    def _():
+        relay((2, 3))
+
     far_relay.wait_recv()
     for slot in range(slots):
         for unit, table in ((own_at, near), (line_at, near_line)):
@@ -220,11 +272,19 @@
             take = slice(part * piece, (part + 1) * piece)
             columns[slot, pair_at[part], :piece] = here[take]
             columns[slot, pair_at[part], piece:] = there[take]
-    relay(1)
-    send_shared(3)
+
+    x_both.wait_recv()
+    cores.append(send(both.at[1, core_me], both.at[1, core_me], core))
+
+    @pl.when(ends)
+    def _():
+        relay((0, 1, 2))
+
+    for copy in diagonal_down:
+        copy.wait_recv()
+    cores.append(send(down.at[3, core_me], down.at[3, core_me], core))
     diagonal_both.wait_recv()
-    diagonal_down.wait_recv()
-    cores += across_core(3)
+    cores.append(send(both.at[3, core_me], both.at[3, core_me], core))
     for copy in cores:
         copy.wait_recv()
 
@@ -266,10 +326,12 @@
             shared[part].wait_recv()
 
         def store(columns_at, value):
-            line_out[number, :, columns_at] = value.astype(jnp.bfloat16)
+            for inside in range(2):
+                line_out[2 * number + inside, :, columns_at] = value[inside * piece : (inside + 1) * piece].astype(jnp.bfloat16)
 
         expert_sum(line_at[number], store)
-        lines.append(send(line_out.at[number], line_in.at[number], line))
+        for part in (2 * number, 2 * number + 1):
+            lines.append(send(line_out.at[part], line_in.at[part], line))
 
     def own_step(number):
         def store(columns_at, value):
@@ -278,28 +340,30 @@
         expert_sum(own_at[number], store)
 
     pair_step(0)
+
+    @pl.when(ends)
+    def _():
+        relay((3,))
+
     pair_step(1)
-    relay(2)
+    own_step(0)
     return_step(0)
+    pair_step(2)
+    return_step(1)
+    pair_step(3)
     line_step(0)
-    return_step(1)
+    return_step(2)
     line_step(1)
-    relay(3)
-    pair_step(2)
-    own_step(0)
-    pair_step(3)
-    return_step(2)
+    return_step(3)
     own_step(1)
-    return_step(3)
-    for number in range(2):
-        lines[number].wait_recv()
-        take = pl.ds(number * batch, batch)
-        own_acc[number] += residual_sc[take].astype(jnp.float32) + line_in[number].astype(jnp.float32)
     for part in range(PARTS):
         returned[part].wait_recv()
+        lines[part].wait_recv()
         inside = pl.ds((part % 2) * piece, piece)
-        value = own_acc[part // 2, inside] + back_in[part].astype(jnp.float32)
-        out_ref[pl.ds(part * piece, piece)] = value.astype(jnp.bfloat16)
+        take = pl.ds(part * piece, piece)
+        value = own_acc[part // 2, inside] + residual_sc[take].astype(jnp.float32)
+        value = value + line_in[part].astype(jnp.float32) + back_in[part].astype(jnp.float32)
+        out_ref[take] = value.astype(jnp.bfloat16)
     for copy in started:
         copy.wait_send()
 
@@ -328,15 +392,24 @@
     piece = rows // PARTS
     wide = slots * cuts * units
     vmem = pl.BlockSpec(memory_space=pltpu.VMEM)
-    hbm = pl.BlockSpec(memory_space=pl.ANY)
+    hbm = pl.BlockSpec(memory_space=pltpu.HBM)
     half = lambda *shape: pltpu.VMEM(shape, jnp.bfloat16)
     single = lambda *shape: pltpu.VMEM(shape, jnp.float32)
     return pl.pallas_call(
         layer_kernel,
-        in_specs=[vmem] * 11 + [hbm] * 3,
+        in_specs=[hbm] * 12 + [vmem] * 2,
         out_specs=vmem,
         out_shape=jax.ShapeDtypeStruct((rows, width), jnp.bfloat16),
         scratch_shapes=[
+            half(*gate_outer.shape),
+            half(*gate_inner.shape),
+            half(*conv_input.shape),
+            half(*conv_taps.shape),
+            half(*out_weight.shape),
+            half(*residual_in.shape),
+            pltpu.VMEM(expert_ids.shape[::-1], jnp.int32),
+            single(1, rows),
+            single(*route_prob.shape[::-1]),
             half(2, HALO_ROWS, channels),
             half(tp, rows + GAIN_ROWS, channels),
             half(tp - 1, rows + GAIN_ROWS, channels),
@@ -352,8 +425,8 @@
             single(slots, 8, 2 * piece, 1),
             half(rows, width),
             single(2, 2 * piece, width),
-            half(2, 2 * piece, width),
-            half(2, 2 * piece, width),
+            half(PARTS, piece, width),
+            half(PARTS, piece, width),
             half(PARTS, piece, width),
             half(PARTS, piece, width),
             single(PARTS, piece, width),
@@ -362,14 +435,14 @@
             half(2 * piece, wide),
             pltpu.SemaphoreType.DMA((COPIES,)),
             pltpu.SemaphoreType.DMA((COPIES,)),
-            pltpu.SemaphoreType.DMA((6,)),
+            pltpu.SemaphoreType.DMA((15,)),
         ],
         compiler_params=pltpu.CompilerParams(
-            collective_id=0, has_side_effects=True, vmem_limit_bytes=56 * 2**20
+            collective_id=0, has_side_effects=True, vmem_limit_bytes=58 * 2**20
         ),
     )(
-        gate_outer, gate_inner, conv_input, conv_taps, norm_gain[None], out_weight, residual_in, moe_gain[None],
-        expert_ids.T, group_prob[None], route_prob.T, expert_gate, expert_up, expert_down,
+        gate_outer, gate_inner, conv_input, conv_taps, out_weight, residual_in, expert_ids.T, group_prob[None],
+        route_prob.T, expert_gate, expert_up, expert_down, norm_gain, moe_gain,
     )
 
 

time: 166 us -> 140 us (0.84)
  Pallas kernels: 161 us -> 138 us
  local copies, waits for them, and re-layouts: 4.84 us -> 2.3 us
    pallas_call x1, Pallas kernels: 161 us -> 138 us  [half_slice(): pl.pallas_call(layer_kernel, in_specs=[hbm] * 12 + [vmem] * 2, out_specs=...]
    broadcast_in_dim x2 -> x0, local copies, waits for them, and re-layouts: 2.53 us -> none  [the longest x1 1.29 us: half_slice(): moe_gain[None]]
where the time goes in v1:
time: 140 us
  Pallas kernels  138 us (99%)
  local copies, waits for them, and re-layouts  2.3 us (2%)
    pallas_call x1, Pallas kernels, half_slice(): pl.pallas_call(layer_kernel, in_specs=[hbm] * 12 + [vmem] * 2, out_specs=...  138 us

profile of v1, /device:TPU:0, one launch (start us, length us, event | category | flops | bytes accessed | tf_op | source)
XLA Modules:
  0.0 140.0 jit_solution(2203923668305424597)
XLA Ops:
  0.0 137.7 %shard_map.136 = bf16[256,2048]{1,0:T(8,128)(2,1)} custom-call(bf16[1024,256]{1,0:T(8,128)(2,1)} %outer_hbm.1, bf16[1024,256]{1,0:T(8,128)(2,1)} %inner_hbm.1, bf16[1024,256]{1,0:T(8,128)(2,1)} %input_hbm.1, bf16[3,256]{1,0:T(4,128)(2,1)} %taps_hbm.1, bf16[256,2048]{1,0:T(8,128)(2,1)} %weight_hbm.1, bf16[256,2048]{1,0:T(8,128)(2,1)} %residual_hbm.1, ...), custom_call_target="tpu_custom_call" | custom-call | tf_op jit(solution)/shard_map/pallas_call | solution.py:398
  137.7 2.3 %copy.16 = bf16[256,2048]{1,0:T(8,128)(2,1)} copy(bf16[256,2048]{1,0:T(8,128)(2,1)} %shard_map.136) | data formatting | bytes 2097152

commit v2 on v1

--- a/solution.py
+++ b/solution.py
@@ -25,7 +25,7 @@
 GAIN_ROWS = 16
 HALO_ROWS = 16
 PARTS = 4
-COPIES = 64
+COPIES = 80
 
 
 def layer_kernel(
@@ -33,7 +33,7 @@
     gate_hbm, up_hbm, down_hbm, gain_ref, moe_ref,
     out_ref,
     outer_ref, inner_ref, input_ref, taps_ref, weight_ref, residual_ref, ids_ref, group_ref, route_ref,
-    halo, sent, got, weights, both, down, tokens, near, far, near_line, far_in, far_line, columns,
+    halo, sent, got, weights, both, down, tokens, near, far, near_side, far_in, far_side, columns,
     residual_sc, own_acc, line_out, line_in, pair_out, pair_in, hold, back_out, back_in, hidden_sc,
     send_sem, recv_sem, local_sem,
 ):
@@ -50,24 +50,25 @@
     after, before = ((sp + 1) % sp_size, tp), ((sp + sp_size - 1) % sp_size, tp)
     peers = [core, line, (sp, lanes[3]), x_peer, z_peer, cross, after, before]
 
+    sources = dict(
+        ids=(ids_hbm, ids_ref), group=(group_hbm, group_ref), route=(route_hbm, route_ref), weight=(weight_hbm, weight_ref),
+        inner=(inner_hbm, inner_ref), input=(input_hbm, input_ref), outer=(outer_hbm, outer_ref), taps=(taps_hbm, taps_ref),
+        residual=(residual_hbm, residual_ref),
+    )
     loaded = {}
-    for number, (name, source, target) in enumerate((
-        ("weight", weight_hbm, weight_ref), ("inner", inner_hbm, inner_ref), ("input", input_hbm, input_ref),
-        ("outer", outer_hbm, outer_ref), ("taps", taps_hbm, taps_ref), ("ids", ids_hbm, ids_ref),
-        ("group", group_hbm, group_ref), ("route", route_hbm, route_ref), ("residual", residual_hbm, residual_ref),
-    )):
-        loaded[name] = pltpu.make_async_copy(source, target, local_sem.at[6 + number])
+    for number, name in enumerate(sources):
+        loaded[name] = pltpu.make_async_copy(*sources[name], local_sem.at[number])
         loaded[name].start()
-
     units = down.shape[2]
     slots, cuts = down.shape[0], down.shape[1]
     fetched = []
     for cut in range(cuts):
-        first = pl.multiple_of((line_me * cuts + cut) * units, units)
+        first = pl.multiple_of((tp ^ cut) * units, units)
+        base = len(sources) + 3 * cut
         fetched += [
-            pltpu.make_async_copy(gate_hbm.at[0, :, pl.ds(first, units)], both.at[0, cut, :, pl.ds(0, units)], local_sem.at[3 * cut]),
-            pltpu.make_async_copy(up_hbm.at[0, :, pl.ds(first, units)], both.at[0, cut, :, pl.ds(units, units)], local_sem.at[3 * cut + 1]),
-            pltpu.make_async_copy(down_hbm.at[0, pl.ds(first, units), :], down.at[0, cut], local_sem.at[3 * cut + 2]),
+            pltpu.make_async_copy(gate_hbm.at[0, :, pl.ds(first, units)], both.at[0, cut, :, pl.ds(0, units)], local_sem.at[base]),
+            pltpu.make_async_copy(up_hbm.at[0, :, pl.ds(first, units)], both.at[0, cut, :, pl.ds(units, units)], local_sem.at[base + 1]),
+            pltpu.make_async_copy(down_hbm.at[0, pl.ds(first, units), :], down.at[0, cut], local_sem.at[base + 2]),
         ]
     for copy in fetched:
         copy.start()
@@ -75,6 +76,19 @@
     barrier = pltpu.get_barrier_semaphore()
     for peer in peers:
         pl.semaphore_signal(barrier, inc=1, device_id=peer, device_id_type=MESH)
+    for name in sources:
+        loaded[name].wait()
+    ids = ids_ref[...]
+    route = route_ref[...]
+    scale = group_ref[...] * route / jnp.sum(route, axis=0, keepdims=True)
+    half = sp_size // 2
+    for number, flip in enumerate((0, 2, 1, 3)):
+        side = (sp % half) ^ flip
+        for table, base in ((near, (sp // half) * half), (far, (1 - sp // half) * half)):
+            chosen = jnp.where(ids == base + side, scale, 0.0)
+            table[number : number + 1, :] = jnp.sum(chosen, axis=0, keepdims=True)
+    for copy in fetched[:3]:
+        copy.wait()
     pl.semaphore_wait(barrier, len(peers))
 
     started = []
@@ -93,8 +107,6 @@
         copy.start()
         return copy
 
-    for name in ("weight", "inner", "input"):
-        loaded[name].wait()
     full = inner_ref.shape[0]
     rows, width = residual_ref.shape
     ends = (sp < 2) | (sp >= sp_size - 2)
@@ -103,38 +115,37 @@
         send(inner_ref.at[pl.ds(full - HALO_ROWS, HALO_ROWS)], halo.at[0], after),
         send(input_ref.at[pl.ds(full - HALO_ROWS, HALO_ROWS)], halo.at[1], after),
     ]
-    quarter = weight_ref.shape[0] // 4
+    strips = 4
+    strip = weight_ref.shape[0] // (2 * strips)
     x_me = sp % 2
 
     def weight_rows(side, number):
-        return pl.ds(pl.multiple_of((2 * side + number) * quarter, quarter), quarter)
+        return pl.ds(pl.multiple_of((strips * side + number) * strip, strip), strip)
 
     weight_line = [
-        send(weight_ref.at[weight_rows(x_me, number)], weights.at[1, weight_rows(x_me, number)], line) for number in range(2)
+        send(weight_ref.at[weight_rows(x_me, number)], weights.at[1, weight_rows(x_me, number)], line) for number in range(strips)
     ]
     weight_core = send(weight_ref, weights.at[0], core)
-    for copy in fetched:
-        copy.wait()
-    unit_half = units // 2
-
-    def down_rows(slot, number):
-        return down.at[slot, core_me, pl.ds(number * unit_half, unit_half)]
-
-    x_down = [send(down_rows(0, 0), down_rows(1, 0), x_peer)]
-    z_both = send(both.at[0, core_me], both.at[2, core_me], z_peer)
-    z_down = send(down.at[0, core_me], down.at[2, core_me], z_peer)
-
-    for name in ("ids", "group", "route", "outer", "taps", "residual"):
-        loaded[name].wait()
-    ids = ids_ref[...]
-    route = route_ref[...]
-    scale = group_ref[...] * route / jnp.sum(route, axis=0, keepdims=True)
-    half = sp_size // 2
-    for slot in range(slots):
-        side = (sp % half) ^ slot
-        for table, base in ((near, (sp // half) * half), (far, (1 - sp // half) * half)):
-            chosen = jnp.where(ids == base + side, scale, 0.0)
-            table[slot : slot + 1, :] = jnp.sum(chosen, axis=0, keepdims=True)
+    far_copy = send(far, far_in, cross)
+    near_copy = send(near, near_side, x_peer)
+    deep, wide = width // 4, units // 2
+
+    def slices(slot, cut):
+        return [both.at[slot, cut, pl.ds(n * deep, deep)] for n in range(4)] + [
+            down.at[slot, cut, pl.ds(n * wide, wide)] for n in range(2)
+        ]
+
+    z_part = [send(source, target, z_peer) for source, target in zip(slices(0, 0), slices(1, 0))]
+    z_core, z_line, z_both = [], [], []
+
+    def z_arrived(number):
+        z_part[number].wait_recv()
+        z_line.append(send(slices(1, 0)[number], slices(1, 2)[number], line))
+        z_core.append(send(slices(1, 0)[number], slices(1, 1)[number], core))
+
+    def line_arrived(number):
+        z_line[number].wait_recv()
+        z_both.append(send(slices(1, 2)[number], slices(1, 3)[number], core))
 
     for copy in halos:
         copy.wait_recv()
@@ -160,8 +171,6 @@
         sent[step, rows:] = jnp.broadcast_to(gain_ref[...].reshape(1, -1), (GAIN_ROWS, mixed.shape[1]))
         if step > 0:
             exchanged.append(send(sent.at[step], got.at[step - 1], (sp, block)))
-    near_copy = send(near, near_line, line)
-    far_copy = send(far, far_in, cross)
 
     piece = rows // PARTS
     batch = 2 * piece
@@ -187,20 +196,22 @@
     partial = squares(blocks[0]) + squares(blocks[1])
 
     weight_x, weight_both = [], []
-    for number in range(2):
+    for number in range(strips):
         weight_line[number].wait_recv()
         arrived = weights.at[1, weight_rows(x_me, number)]
         weight_x.append(send(arrived, arrived, x_peer))
         weight_both.append(send(arrived, weights.at[2, weight_rows(x_me, number)], core))
-    x_down.append(send(down_rows(0, 1), down_rows(1, 1), x_peer))
-    x_both = send(both.at[0, core_me], both.at[1, core_me], x_peer)
-    x_down[0].wait_recv()
-    diagonal_down = [send(down_rows(1, 0), down_rows(3, 0), z_peer)]
-    for number in range(2):
+    z_arrived(0)
+    z_arrived(1)
+    for number in range(strips):
         weight_x[number].wait_recv()
         arrived = weights.at[1, weight_rows(1 - x_me, number)]
         weight_both.append(send(arrived, weights.at[2, weight_rows(1 - x_me, number)], core))
 
+    z_arrived(2)
+    far_copy.wait_recv()
+    far_relay = send(far_in, far_side, x_peer)
+    near_copy.wait_recv()
     for copy in exchanged[:2]:
         copy.wait_recv()
     total = partial + squares(blocks[2]) + squares(blocks[3])
@@ -229,63 +240,45 @@
         return tokens.at[pair_at[part], pl.ds(second * piece, piece)]
 
     across = [send(own_rows(part), pair_rows(part, 0), cross) for part in range(PARTS)]
-    shared = [prepare(own_rows(part), line_rows(part), line) for part in range(PARTS)]
-    beside = [prepare(pair_rows(part, 0), pair_rows(part, 1), line) for part in range(PARTS)]
-    for copy in shared:
-        copy.start()
-
-    def relay(parts):
-        for part in parts:
-            across[part].wait_recv()
-            beside[part].start()
-
-    far_copy.wait_recv()
-    far_relay = send(far_in, far_line, line)
-    near_copy.wait_recv()
-
-    z_both.wait_recv()
-    diagonal_both = send(both.at[2, core_me], both.at[3, core_me], x_peer)
-    cores = [send(both.at[2, core_me], both.at[2, core_me], core)]
-    x_down[1].wait_recv()
-    diagonal_down.append(send(down_rows(1, 1), down_rows(3, 1), z_peer))
-    cores.append(send(down.at[1, core_me], down.at[1, core_me], core))
-
-    @pl.when(middle)
-    def _():
-        relay((0, 1))
-
-    z_down.wait_recv()
-    cores.append(send(down.at[2, core_me], down.at[2, core_me], core))
-
-    @pl.when(middle)
-    def _():
-        relay((2, 3))
-
+    shared = [send(own_rows(part), line_rows(part), x_peer) for part in range(PARTS)]
+    beside = [prepare(pair_rows(part, 0), pair_rows(part, 1), x_peer) for part in range(PARTS)]
+
+    def relay(part):
+        across[part].wait_recv()
+        beside[part].start()
+
+    def only(where, action, *arguments):
+        @pl.when(where)
+        def _():
+            for argument in arguments:
+                action(argument)
+
+    z_arrived(3)
+    line_arrived(0)
+    only(ends, relay, 0)
+    z_arrived(4)
+    line_arrived(1)
+    only(ends, relay, 1)
     far_relay.wait_recv()
     for slot in range(slots):
-        for unit, table in ((own_at, near), (line_at, near_line)):
-            column = table[slot : slot + 1, :].T
+        for unit, table, row in ((own_at, near, slot), (line_at, near_side, slots + slot)):
+            column = table[row : row + 1, :].T
             for number in range(2):
                 columns[slot, unit[number]] = column[number * batch : (number + 1) * batch]
-        here, there = far_in[slot : slot + 1, :].T, far_line[slot : slot + 1, :].T
+        here, there = far_in[slot : slot + 1, :].T, far_side[slots + slot : slots + slot + 1, :].T
         for part in range(PARTS):
             take = slice(part * piece, (part + 1) * piece)
             columns[slot, pair_at[part], :piece] = here[take]
             columns[slot, pair_at[part], piece:] = there[take]
-
-    x_both.wait_recv()
-    cores.append(send(both.at[1, core_me], both.at[1, core_me], core))
-
-    @pl.when(ends)
-    def _():
-        relay((0, 1, 2))
-
-    for copy in diagonal_down:
-        copy.wait_recv()
-    cores.append(send(down.at[3, core_me], down.at[3, core_me], core))
-    diagonal_both.wait_recv()
-    cores.append(send(both.at[3, core_me], both.at[3, core_me], core))
-    for copy in cores:
+    line_arrived(2)
+    line_arrived(3)
+    only(middle, relay, 0, 1)
+    z_arrived(5)
+    line_arrived(4)
+    line_arrived(5)
+    for copy in fetched[3:]:
+        copy.wait()
+    for copy in z_core + z_both:
         copy.wait_recv()
 
     def expert_sum(unit, store):
@@ -314,7 +307,7 @@
             pair_out[part, :, columns_at] = value[piece:].astype(jnp.bfloat16)
 
         expert_sum(pair_at[part], store)
-        pairs.append(send(pair_out.at[part], pair_in.at[part], line))
+        pairs.append(send(pair_out.at[part], pair_in.at[part], x_peer))
 
     def return_step(part):
         pairs[part].wait_recv()
@@ -331,7 +324,7 @@
 
         expert_sum(line_at[number], store)
         for part in (2 * number, 2 * number + 1):
-            lines.append(send(line_out.at[part], line_in.at[part], line))
+            lines.append(send(line_out.at[part], line_in.at[part], x_peer))
 
     def own_step(number):
         def store(columns_at, value):
@@ -340,22 +333,21 @@
         expert_sum(own_at[number], store)
 
     pair_step(0)
-
-    @pl.when(ends)
-    def _():
-        relay((3,))
-
+    only(middle, relay, 2)
     pair_step(1)
+    only(middle, relay, 3)
     own_step(0)
     return_step(0)
+    only(ends, relay, 2)
+    return_step(1)
+    only(ends, relay, 3)
     pair_step(2)
-    return_step(1)
+    own_step(1)
     pair_step(3)
+    return_step(2)
     line_step(0)
-    return_step(2)
+    return_step(3)
     line_step(1)
-    return_step(3)
-    own_step(1)
     for part in range(PARTS):
         returned[part].wait_recv()
         lines[part].wait_recv()
@@ -387,7 +379,7 @@
     sp, tp = lax.axis_size("sp"), lax.axis_size("tp")
     rows, width = residual_in.shape
     channels = gate_outer.shape[1]
-    slots, cuts = sp // 2, 2
+    slots, cuts = 2, tp
     units = expert_gate.shape[2] // tp
     piece = rows // PARTS
     wide = slots * cuts * units
@@ -417,11 +409,11 @@
             half(slots, cuts, width, 2 * units),
             half(slots, cuts, units, width),
             half(8, 2 * piece, width),
-            single(slots, rows),
-            single(slots, rows),
-            single(slots, rows),
-            single(slots, rows),
-            single(slots, rows),
+            single(2 * slots, rows),
+            single(2 * slots, rows),
+            single(2 * slots, rows),
+            single(2 * slots, rows),
+            single(2 * slots, rows),
             single(slots, 8, 2 * piece, 1),
             half(rows, width),
             single(2, 2 * piece, width),
@@ -435,7 +427,7 @@
             half(2 * piece, wide),
             pltpu.SemaphoreType.DMA((COPIES,)),
             pltpu.SemaphoreType.DMA((COPIES,)),
-            pltpu.SemaphoreType.DMA((15,)),
+            pltpu.SemaphoreType.DMA((9 + 3 * cuts,)),
         ],
         compiler_params=pltpu.CompilerParams(
             collective_id=0, has_side_effects=True, vmem_limit_bytes=58 * 2**20

time: 140 us -> 130 us (0.929)
  Pallas kernels: 138 us -> 127 us
    pallas_call x1, Pallas kernels: 138 us -> 127 us  [half_slice(): pl.pallas_call(layer_kernel, in_specs=[hbm] * 12 + [vmem] * 2, out_specs=...]
where the time goes in v2:
time: 130 us; the launch traced here: 129 us
  Pallas kernels  127 us (98%)
  local copies, waits for them, and re-layouts  2.3 us (2%)
    pallas_call x1, Pallas kernels, half_slice(): pl.pallas_call(layer_kernel, in_specs=[hbm] * 12 + [vmem] * 2, out_specs=...  127 us

profile of v2, /device:TPU:0, one launch (start us, length us, event | category | flops | bytes accessed | tf_op | source)
XLA Modules:
  0.0 129.5 jit_solution(16165787655974479252)
XLA Ops:
  0.0 127.2 %shard_map.136 = bf16[256,2048]{1,0:T(8,128)(2,1)} custom-call(bf16[1024,256]{1,0:T(8,128)(2,1)} %outer_hbm.1, bf16[1024,256]{1,0:T(8,128)(2,1)} %inner_hbm.1, bf16[1024,256]{1,0:T(8,128)(2,1)} %input_hbm.1, bf16[3,256]{1,0:T(4,128)(2,1)} %taps_hbm.1, bf16[256,2048]{1,0:T(8,128)(2,1)} %weight_hbm.1, bf16[256,2048]{1,0:T(8,128)(2,1)} %residual_hbm.1, ...), custom_call_target="tpu_custom_call" | custom-call | tf_op jit(solution)/shard_map/pallas_call | solution.py:390
  127.2 2.3 %copy.16 = bf16[256,2048]{1,0:T(8,128)(2,1)} copy(bf16[256,2048]{1,0:T(8,128)(2,1)} %shard_map.136) | data formatting | bytes 2097152

commit v3 on v2

--- a/solution.py
+++ b/solution.py
@@ -25,16 +25,16 @@
 GAIN_ROWS = 16
 HALO_ROWS = 16
 PARTS = 4
-COPIES = 80
+COPIES = 67
 
 
 def layer_kernel(
     outer_hbm, inner_hbm, input_hbm, taps_hbm, weight_hbm, residual_hbm, ids_hbm, group_hbm, route_hbm,
     gate_hbm, up_hbm, down_hbm, gain_ref, moe_ref,
-    out_ref,
+    out_hbm,
     outer_ref, inner_ref, input_ref, taps_ref, weight_ref, residual_ref, ids_ref, group_ref, route_ref,
     halo, sent, got, weights, both, down, tokens, near, far, near_side, far_in, far_side, columns,
-    residual_sc, own_acc, line_out, line_in, pair_out, pair_in, hold, back_out, back_in, hidden_sc,
+    residual_sc, own_acc, line_out, line_in, pair_out, pair_in, hold, back_out, back_in, hidden_sc, final,
     send_sem, recv_sem, local_sem,
 ):
     sp, tp = lax.axis_index("sp"), lax.axis_index("tp")
@@ -50,33 +50,68 @@
     after, before = ((sp + 1) % sp_size, tp), ((sp + sp_size - 1) % sp_size, tp)
     peers = [core, line, (sp, lanes[3]), x_peer, z_peer, cross, after, before]
 
-    sources = dict(
-        ids=(ids_hbm, ids_ref), group=(group_hbm, group_ref), route=(route_hbm, route_ref), weight=(weight_hbm, weight_ref),
-        inner=(inner_hbm, inner_ref), input=(input_hbm, input_ref), outer=(outer_hbm, outer_ref), taps=(taps_hbm, taps_ref),
-        residual=(residual_hbm, residual_ref),
-    )
-    loaded = {}
-    for number, name in enumerate(sources):
-        loaded[name] = pltpu.make_async_copy(*sources[name], local_sem.at[number])
-        loaded[name].start()
+    barrier = pltpu.get_barrier_semaphore()
+    for peer in peers:
+        pl.semaphore_signal(barrier, inc=1, device_id=peer, device_id_type=MESH)
     units = down.shape[2]
     slots, cuts = down.shape[0], down.shape[1]
     fetched = []
     for cut in range(cuts):
         first = pl.multiple_of((tp ^ cut) * units, units)
-        base = len(sources) + 3 * cut
         fetched += [
-            pltpu.make_async_copy(gate_hbm.at[0, :, pl.ds(first, units)], both.at[0, cut, :, pl.ds(0, units)], local_sem.at[base]),
-            pltpu.make_async_copy(up_hbm.at[0, :, pl.ds(first, units)], both.at[0, cut, :, pl.ds(units, units)], local_sem.at[base + 1]),
-            pltpu.make_async_copy(down_hbm.at[0, pl.ds(first, units), :], down.at[0, cut], local_sem.at[base + 2]),
+            pltpu.make_async_copy(gate_hbm.at[0, :, pl.ds(first, units)], both.at[0, cut, :, pl.ds(0, units)], local_sem.at[3 * cut]),
+            pltpu.make_async_copy(up_hbm.at[0, :, pl.ds(first, units)], both.at[0, cut, :, pl.ds(units, units)], local_sem.at[3 * cut + 1]),
+            pltpu.make_async_copy(down_hbm.at[0, pl.ds(first, units), :], down.at[0, cut], local_sem.at[3 * cut + 2]),
         ]
-    for copy in fetched:
+    for copy in fetched[:3]:
         copy.start()
-
-    barrier = pltpu.get_barrier_semaphore()
-    for peer in peers:
-        pl.semaphore_signal(barrier, inc=1, device_id=peer, device_id_type=MESH)
-    for name in sources:
+    sources = dict(
+        ids=(ids_hbm, ids_ref), group=(group_hbm, group_ref), route=(route_hbm, route_ref), inner=(inner_hbm, inner_ref),
+        input=(input_hbm, input_ref), outer=(outer_hbm, outer_ref), taps=(taps_hbm, taps_ref), weight=(weight_hbm, weight_ref),
+        residual=(residual_hbm, residual_ref),
+    )
+    loaded = {}
+    for number, name in enumerate(sources):
+        loaded[name] = pltpu.make_async_copy(*sources[name], local_sem.at[3 * cuts + number])
+        loaded[name].start()
+    pl.semaphore_wait(barrier, len(peers))
+
+    started = []
+
+    def prepare(source, target, peer):
+        number = len(started)
+        copy = pltpu.make_async_remote_copy(
+            src_ref=source, dst_ref=target, send_sem=send_sem.at[number], recv_sem=recv_sem.at[number],
+            device_id=peer, device_id_type=MESH,
+        )
+        started.append(copy)
+        return copy
+
+    def send(source, target, peer):
+        copy = prepare(source, target, peer)
+        copy.start()
+        return copy
+
+    full = inner_ref.shape[0]
+    rows, width = residual_ref.shape
+    ends = (sp < 2) | (sp >= sp_size - 2)
+    middle = jnp.logical_not(ends)
+    halos = [
+        send(inner_hbm.at[pl.ds(full - HALO_ROWS, HALO_ROWS)], halo.at[0], after),
+        send(input_hbm.at[pl.ds(full - HALO_ROWS, HALO_ROWS)], halo.at[1], after),
+    ]
+    strips = 4
+    strip = weight_ref.shape[0] // (2 * strips)
+    x_me = sp % 2
+
+    def weight_rows(side, number):
+        return pl.ds(pl.multiple_of((strips * side + number) * strip, strip), strip)
+
+    weight_line = [
+        send(weight_hbm.at[weight_rows(x_me, number)], weights.at[1, weight_rows(x_me, number)], line) for number in range(strips)
+    ]
+    weight_core = send(weight_hbm, weights.at[0], core)
+    for name in ("ids", "group", "route"):
         loaded[name].wait()
     ids = ids_ref[...]
     route = route_ref[...]
@@ -87,65 +122,50 @@
         for table, base in ((near, (sp // half) * half), (far, (1 - sp // half) * half)):
             chosen = jnp.where(ids == base + side, scale, 0.0)
             table[number : number + 1, :] = jnp.sum(chosen, axis=0, keepdims=True)
+    far_copy = send(far, far_in, cross)
+    near_copy = send(near, near_side, x_peer)
+    deep, wide = width // 4, units // 4
+
+    def slices(slot, cut):
+        return [both.at[slot, cut, pl.ds(n * deep, deep)] for n in range(4)] + [
+            down.at[slot, cut, pl.ds(n * wide, wide)] for n in range(4)
+        ]
+
     for copy in fetched[:3]:
         copy.wait()
-    pl.semaphore_wait(barrier, len(peers))
-
-    started = []
-
-    def prepare(source, target, peer):
-        number = len(started)
-        copy = pltpu.make_async_remote_copy(
-            src_ref=source, dst_ref=target, send_sem=send_sem.at[number], recv_sem=recv_sem.at[number],
-            device_id=peer, device_id_type=MESH,
-        )
-        started.append(copy)
-        return copy
-
-    def send(source, target, peer):
-        copy = prepare(source, target, peer)
+    z_part = [prepare(source, target, z_peer) for source, target in zip(slices(0, 0), slices(1, 0))]
+
+    def only(where, action, *arguments):
+        @pl.when(where)
+        def _():
+            for argument in arguments:
+                action(argument)
+
+    for copy in z_part[:4]:
         copy.start()
-        return copy
-
-    full = inner_ref.shape[0]
-    rows, width = residual_ref.shape
-    ends = (sp < 2) | (sp >= sp_size - 2)
-    middle = jnp.logical_not(ends)
-    halos = [
-        send(inner_ref.at[pl.ds(full - HALO_ROWS, HALO_ROWS)], halo.at[0], after),
-        send(input_ref.at[pl.ds(full - HALO_ROWS, HALO_ROWS)], halo.at[1], after),
-    ]
-    strips = 4
-    strip = weight_ref.shape[0] // (2 * strips)
-    x_me = sp % 2
-
-    def weight_rows(side, number):
-        return pl.ds(pl.multiple_of((strips * side + number) * strip, strip), strip)
-
-    weight_line = [
-        send(weight_ref.at[weight_rows(x_me, number)], weights.at[1, weight_rows(x_me, number)], line) for number in range(strips)
-    ]
-    weight_core = send(weight_ref, weights.at[0], core)
-    far_copy = send(far, far_in, cross)
-    near_copy = send(near, near_side, x_peer)
-    deep, wide = width // 4, units // 2
-
-    def slices(slot, cut):
-        return [both.at[slot, cut, pl.ds(n * deep, deep)] for n in range(4)] + [
-            down.at[slot, cut, pl.ds(n * wide, wide)] for n in range(2)
-        ]
-
-    z_part = [send(source, target, z_peer) for source, target in zip(slices(0, 0), slices(1, 0))]
+    only(middle, lambda number: z_part[number].start(), 4, 5, 6, 7)
+    for copy in fetched[3:]:
+        copy.start()
     z_core, z_line, z_both = [], [], []
+
+    def beyond(cut, target, number, sends):
+        pair = pl.ds((number // 2) * 2 * deep, 2 * deep)
+        if number in (1, 3):
+            sends.append(send(both.at[1, cut, pair], both.at[1, target, pair], core))
+        if number == 7:
+            sends.append(send(down.at[1, cut], down.at[1, target], core))
 
     def z_arrived(number):
         z_part[number].wait_recv()
         z_line.append(send(slices(1, 0)[number], slices(1, 2)[number], line))
-        z_core.append(send(slices(1, 0)[number], slices(1, 1)[number], core))
+        beyond(0, 1, number, z_core)
 
     def line_arrived(number):
         z_line[number].wait_recv()
-        z_both.append(send(slices(1, 2)[number], slices(1, 3)[number], core))
+        beyond(2, 3, number, z_both)
+
+    for name in ("inner", "input", "outer", "taps"):
+        loaded[name].wait()
 
     for copy in halos:
         copy.wait_recv()
@@ -190,25 +210,30 @@
 
     exchanged[2].wait_recv()
     weight_core.wait_recv()
+    loaded["weight"].wait()
+    loaded["residual"].wait()
     for number in range(2):
         take = slice(number * batch, (number + 1) * batch)
         own_acc[number] = product(0, take) + product(1, take)
     partial = squares(blocks[0]) + squares(blocks[1])
 
     weight_x, weight_both = [], []
+
+    def weight_pair(side, number):
+        if number % 2 == 1:
+            rows_at = pl.ds(pl.multiple_of((strips * side + number - 1) * strip, 2 * strip), 2 * strip)
+            weight_both.append(send(weights.at[1, rows_at], weights.at[2, rows_at], core))
+
     for number in range(strips):
         weight_line[number].wait_recv()
         arrived = weights.at[1, weight_rows(x_me, number)]
         weight_x.append(send(arrived, arrived, x_peer))
-        weight_both.append(send(arrived, weights.at[2, weight_rows(x_me, number)], core))
+        weight_pair(x_me, number)
     z_arrived(0)
     z_arrived(1)
     for number in range(strips):
         weight_x[number].wait_recv()
-        arrived = weights.at[1, weight_rows(1 - x_me, number)]
-        weight_both.append(send(arrived, weights.at[2, weight_rows(1 - x_me, number)], core))
-
-    z_arrived(2)
+        weight_pair(1 - x_me, number)
     far_copy.wait_recv()
     far_relay = send(far_in, far_side, x_peer)
     near_copy.wait_recv()
@@ -219,6 +244,16 @@
     for copy in weight_both:
         copy.wait_recv()
     own_at, line_at, pair_at = (4, 5), (2, 3), (0, 1, 6, 7)
+    def own_rows(part):
+        return tokens.at[own_at[part // 2], pl.ds((part % 2) * piece, piece)]
+
+    def line_rows(part):
+        return tokens.at[line_at[part // 2], pl.ds((part % 2) * piece, piece)]
+
+    def pair_rows(part, second):
+        return tokens.at[pair_at[part], pl.ds(second * piece, piece)]
+
+    across, shared = [], []
     for number, unit in enumerate(own_at):
         take = slice(number * batch, (number + 1) * batch)
         projected = own_acc[number] + product(2, take) + product(3, take)
@@ -229,36 +264,27 @@
         mean = jnp.mean(floats * floats, axis=1, keepdims=True)
         routed = floats * lax.rsqrt(mean + EPSILON) * moe_ref[...].reshape(1, -1).astype(jnp.float32)
         tokens[unit] = routed.astype(jnp.bfloat16)
-
-    def own_rows(part):
-        return tokens.at[own_at[part // 2], pl.ds((part % 2) * piece, piece)]
-
-    def line_rows(part):
-        return tokens.at[line_at[part // 2], pl.ds((part % 2) * piece, piece)]
-
-    def pair_rows(part, second):
-        return tokens.at[pair_at[part], pl.ds(second * piece, piece)]
-
-    across = [send(own_rows(part), pair_rows(part, 0), cross) for part in range(PARTS)]
-    shared = [send(own_rows(part), line_rows(part), x_peer) for part in range(PARTS)]
+        for part in (2 * number, 2 * number + 1):
+            across.append(send(own_rows(part), pair_rows(part, 0), cross))
+            shared.append(send(own_rows(part), line_rows(part), x_peer))
+        if number == 0:
+            only(ends, lambda number: z_part[number].start(), 4, 5, 6, 7)
+
     beside = [prepare(pair_rows(part, 0), pair_rows(part, 1), x_peer) for part in range(PARTS)]
 
     def relay(part):
         across[part].wait_recv()
         beside[part].start()
 
-    def only(where, action, *arguments):
-        @pl.when(where)
-        def _():
-            for argument in arguments:
-                action(argument)
-
+    z_arrived(2)
+    line_arrived(0)
     z_arrived(3)
-    line_arrived(0)
-    only(ends, relay, 0)
+    line_arrived(1)
+    only(middle, relay, 0, 1)
     z_arrived(4)
-    line_arrived(1)
-    only(ends, relay, 1)
+    z_arrived(5)
+    line_arrived(2)
+    only(ends, relay, 0, 1)
     far_relay.wait_recv()
     for slot in range(slots):
         for unit, table, row in ((own_at, near, slot), (line_at, near_side, slots + slot)):
@@ -270,12 +296,11 @@
             take = slice(part * piece, (part + 1) * piece)
             columns[slot, pair_at[part], :piece] = here[take]
             columns[slot, pair_at[part], piece:] = there[take]
-    line_arrived(2)
+    z_arrived(6)
+    z_arrived(7)
     line_arrived(3)
-    only(middle, relay, 0, 1)
-    z_arrived(5)
-    line_arrived(4)
-    line_arrived(5)
+    for number in range(4, 8):
+        line_arrived(number)
     for copy in fetched[3:]:
         copy.wait()
     for copy in z_core + z_both:
@@ -337,10 +362,9 @@
     pair_step(1)
     only(middle, relay, 3)
     own_step(0)
+    only(ends, relay, 2, 3)
     return_step(0)
-    only(ends, relay, 2)
     return_step(1)
-    only(ends, relay, 3)
     pair_step(2)
     own_step(1)
     pair_step(3)
@@ -348,6 +372,11 @@
     line_step(0)
     return_step(3)
     line_step(1)
+    late = pairs + lines + returned
+    for copy in started:
+        if all(copy is not other for other in late):
+            copy.wait_send()
+    written = []
     for part in range(PARTS):
         returned[part].wait_recv()
         lines[part].wait_recv()
@@ -355,9 +384,13 @@
         take = pl.ds(part * piece, piece)
         value = own_acc[part // 2, inside] + residual_sc[take].astype(jnp.float32)
         value = value + line_in[part].astype(jnp.float32) + back_in[part].astype(jnp.float32)
-        out_ref[take] = value.astype(jnp.bfloat16)
-    for copy in started:
+        final[part] = value.astype(jnp.bfloat16)
+        written.append(pltpu.make_async_copy(final.at[part], out_hbm.at[take], local_sem.at[part]))
+        written[part].start()
+    for copy in late:
         copy.wait_send()
+    for copy in written:
+        copy.wait()
 
 
 def half_slice(
@@ -390,7 +423,7 @@
     return pl.pallas_call(
         layer_kernel,
         in_specs=[hbm] * 12 + [vmem] * 2,
-        out_specs=vmem,
+        out_specs=hbm,
         out_shape=jax.ShapeDtypeStruct((rows, width), jnp.bfloat16),
         scratch_shapes=[
             half(*gate_outer.shape),
@@ -425,6 +458,7 @@
             half(PARTS, piece, width),
             half(PARTS, piece, width),
             half(2 * piece, wide),
+            half(PARTS, piece, width),
             pltpu.SemaphoreType.DMA((COPIES,)),
             pltpu.SemaphoreType.DMA((COPIES,)),
             pltpu.SemaphoreType.DMA((9 + 3 * cuts,)),

time: 130 us -> 125 us (0.962)
  Pallas kernels: 127 us -> 122 us
    pallas_call x1, Pallas kernels: 127 us -> 122 us  [half_slice(): pl.pallas_call(layer_kernel, in_specs=[hbm] * 12 + [vmem] * 2, out_specs=...]
where the time goes in v3:
time: 125 us; the launch traced here: 124 us
  Pallas kernels  122 us (98%)
  local copies, waits for them, and re-layouts  2.3 us (2%)
    pallas_call x1, Pallas kernels, half_slice(): pl.pallas_call(layer_kernel, in_specs=[hbm] * 12 + [vmem] * 2, out_specs=...  122 us

profile of v3, /device:TPU:0, one launch (start us, length us, event | category | flops | bytes accessed | tf_op | source)
XLA Modules:
  0.0 123.8 jit_solution(2114593570318822239)
XLA Ops:
  0.0 121.5 %shard_map.136 = bf16[256,2048]{1,0:T(8,128)(2,1)} custom-call(bf16[1024,256]{1,0:T(8,128)(2,1)} %outer_hbm.1, bf16[1024,256]{1,0:T(8,128)(2,1)} %inner_hbm.1, bf16[1024,256]{1,0:T(8,128)(2,1)} %input_hbm.1, bf16[3,256]{1,0:T(4,128)(2,1)} %taps_hbm.1, bf16[256,2048]{1,0:T(8,128)(2,1)} %weight_hbm.1, bf16[256,2048]{1,0:T(8,128)(2,1)} %residual_hbm.1, ...), custom_call_target="tpu_custom_call" | custom-call | tf_op jit(solution)/shard_map/pallas_call | solution.py:423
  121.5 2.3 %copy.16 = bf16[256,2048]{1,0:T(8,128)(2,1)} copy(bf16[256,2048]{1,0:T(8,128)(2,1)} %shard_map.136) | data formatting | bytes 2097152

commit v4 on v3

--- a/solution.py
+++ b/solution.py
@@ -30,9 +30,9 @@
 
 def layer_kernel(
     outer_hbm, inner_hbm, input_hbm, taps_hbm, weight_hbm, residual_hbm, ids_hbm, group_hbm, route_hbm,
-    gate_hbm, up_hbm, down_hbm, gain_ref, moe_ref,
+    gate_hbm, up_hbm, down_hbm, gain_hbm, moe_hbm,
     out_hbm,
-    outer_ref, inner_ref, input_ref, taps_ref, weight_ref, residual_ref, ids_ref, group_ref, route_ref,
+    outer_ref, inner_ref, input_ref, taps_ref, weight_ref, residual_ref, ids_ref, group_ref, route_ref, gain_ref, moe_ref,
     halo, sent, got, weights, both, down, tokens, near, far, near_side, far_in, far_side, columns,
     residual_sc, own_acc, line_out, line_in, pair_out, pair_in, hold, back_out, back_in, hidden_sc, final,
     send_sem, recv_sem, local_sem,
@@ -48,11 +48,17 @@
     z_peer = (sp + 2 - 4 * ((sp // 2) % 2), tp)
     cross = ((sp + sp_size // 2) % sp_size, tp)
     after, before = ((sp + 1) % sp_size, tp), ((sp + sp_size - 1) % sp_size, tp)
-    peers = [core, line, (sp, lanes[3]), x_peer, z_peer, cross, after, before]
+    peers = [core, line, (sp, lanes[3]), x_peer, z_peer, cross]
+    first_block, last_block = sp == 0, sp == sp_size - 1
 
     barrier = pltpu.get_barrier_semaphore()
     for peer in peers:
         pl.semaphore_signal(barrier, inc=1, device_id=peer, device_id_type=MESH)
+    for absent, peer in ((last_block, after), (first_block, before)):
+        @pl.when(jnp.logical_not(absent))
+        def _():
+            pl.semaphore_signal(barrier, inc=1, device_id=peer, device_id_type=MESH)
+
     units = down.shape[2]
     slots, cuts = down.shape[0], down.shape[1]
     fetched = []
@@ -68,13 +74,13 @@
     sources = dict(
         ids=(ids_hbm, ids_ref), group=(group_hbm, group_ref), route=(route_hbm, route_ref), inner=(inner_hbm, inner_ref),
         input=(input_hbm, input_ref), outer=(outer_hbm, outer_ref), taps=(taps_hbm, taps_ref), weight=(weight_hbm, weight_ref),
-        residual=(residual_hbm, residual_ref),
+        gain=(gain_hbm, gain_ref), moe=(moe_hbm, moe_ref), residual=(residual_hbm, residual_ref),
     )
     loaded = {}
     for number, name in enumerate(sources):
         loaded[name] = pltpu.make_async_copy(*sources[name], local_sem.at[3 * cuts + number])
         loaded[name].start()
-    pl.semaphore_wait(barrier, len(peers))
+    pl.semaphore_wait(barrier, jnp.where(first_block | last_block, len(peers) + 1, len(peers) + 2))
 
     started = []
 
@@ -97,9 +103,17 @@
     ends = (sp < 2) | (sp >= sp_size - 2)
     middle = jnp.logical_not(ends)
     halos = [
-        send(inner_hbm.at[pl.ds(full - HALO_ROWS, HALO_ROWS)], halo.at[0], after),
-        send(input_hbm.at[pl.ds(full - HALO_ROWS, HALO_ROWS)], halo.at[1], after),
+        prepare(inner_hbm.at[pl.ds(full - HALO_ROWS, HALO_ROWS)], halo.at[0], after),
+        prepare(input_hbm.at[pl.ds(full - HALO_ROWS, HALO_ROWS)], halo.at[1], after),
     ]
+
+    def only(where, action, *arguments):
+        @pl.when(where)
+        def _():
+            for argument in arguments:
+                action(argument)
+
+    only(jnp.logical_not(last_block), lambda copy: copy.start(), *halos)
     strips = 4
     strip = weight_ref.shape[0] // (2 * strips)
     x_me = sp % 2
@@ -111,6 +125,17 @@
         send(weight_hbm.at[weight_rows(x_me, number)], weights.at[1, weight_rows(x_me, number)], line) for number in range(strips)
     ]
     weight_core = send(weight_hbm, weights.at[0], core)
+    deep, wide = width // 4, units // 4
+
+    def slices(slot, cut):
+        return [both.at[slot, cut, pl.ds(n * deep, deep)] for n in range(4)] + [
+            down.at[slot, cut, pl.ds(n * wide, wide)] for n in range(4)
+        ]
+
+    z_part = [prepare(source, target, z_peer) for source, target in zip(slices(0, 0), slices(1, 0))]
+    for copy in fetched[:2]:
+        copy.wait()
+    z_part[0].start()
     for name in ("ids", "group", "route"):
         loaded[name].wait()
     ids = ids_ref[...]
@@ -124,25 +149,9 @@
             table[number : number + 1, :] = jnp.sum(chosen, axis=0, keepdims=True)
     far_copy = send(far, far_in, cross)
     near_copy = send(near, near_side, x_peer)
-    deep, wide = width // 4, units // 4
-
-    def slices(slot, cut):
-        return [both.at[slot, cut, pl.ds(n * deep, deep)] for n in range(4)] + [
-            down.at[slot, cut, pl.ds(n * wide, wide)] for n in range(4)
-        ]
-
-    for copy in fetched[:3]:
-        copy.wait()
-    z_part = [prepare(source, target, z_peer) for source, target in zip(slices(0, 0), slices(1, 0))]
-
-    def only(where, action, *arguments):
-        @pl.when(where)
-        def _():
-            for argument in arguments:
-                action(argument)
-
-    for copy in z_part[:4]:
+    for copy in z_part[1:4]:
         copy.start()
+    fetched[2].wait()
     only(middle, lambda number: z_part[number].start(), 4, 5, 6, 7)
     for copy in fetched[3:]:
         copy.start()
@@ -164,11 +173,10 @@
         z_line[number].wait_recv()
         beyond(2, 3, number, z_both)
 
-    for name in ("inner", "input", "outer", "taps"):
+    for name in ("inner", "input", "outer", "taps", "gain", "moe"):
         loaded[name].wait()
 
-    for copy in halos:
-        copy.wait_recv()
+    only(jnp.logical_not(first_block), lambda copy: copy.wait_recv(), *halos)
     taps = taps_ref[...].astype(jnp.float32)
     count = taps.shape[0]
     exchanged = []
@@ -372,7 +380,8 @@
     line_step(0)
     return_step(3)
     line_step(1)
-    late = pairs + lines + returned
+    late = pairs + lines + returned + halos
+    only(jnp.logical_not(last_block), lambda copy: copy.wait_send(), *halos)
     for copy in started:
         if all(copy is not other for other in late):
             copy.wait_send()
@@ -387,7 +396,7 @@
         final[part] = value.astype(jnp.bfloat16)
         written.append(pltpu.make_async_copy(final.at[part], out_hbm.at[take], local_sem.at[part]))
         written[part].start()
-    for copy in late:
+    for copy in pairs + lines + returned:
         copy.wait_send()
     for copy in written:
         copy.wait()
@@ -416,13 +425,12 @@
     units = expert_gate.shape[2] // tp
     piece = rows // PARTS
     wide = slots * cuts * units
-    vmem = pl.BlockSpec(memory_space=pltpu.VMEM)
     hbm = pl.BlockSpec(memory_space=pltpu.HBM)
     half = lambda *shape: pltpu.VMEM(shape, jnp.bfloat16)
     single = lambda *shape: pltpu.VMEM(shape, jnp.float32)
     return pl.pallas_call(
         layer_kernel,
-        in_specs=[hbm] * 12 + [vmem] * 2,
+        in_specs=[hbm] * 14,
         out_specs=hbm,
         out_shape=jax.ShapeDtypeStruct((rows, width), jnp.bfloat16),
         scratch_shapes=[
@@ -435,6 +443,8 @@
             pltpu.VMEM(expert_ids.shape[::-1], jnp.int32),
             single(1, rows),
             single(*route_prob.shape[::-1]),
+            half(*norm_gain.shape),
+            half(*moe_gain.shape),
             half(2, HALO_ROWS, channels),
             half(tp, rows + GAIN_ROWS, channels),
             half(tp - 1, rows + GAIN_ROWS, channels),
@@ -461,7 +471,7 @@
             half(PARTS, piece, width),
             pltpu.SemaphoreType.DMA((COPIES,)),
             pltpu.SemaphoreType.DMA((COPIES,)),
-            pltpu.SemaphoreType.DMA((9 + 3 * cuts,)),
+            pltpu.SemaphoreType.DMA((11 + 3 * cuts,)),
         ],
         compiler_params=pltpu.CompilerParams(
             collective_id=0, has_side_effects=True, vmem_limit_bytes=58 * 2**20

time: 125 us -> 123 us (0.984)
  Pallas kernels: 122 us -> 120 us
    pallas_call x1, Pallas kernels: 122 us -> 120 us  [half_slice(): pl.pallas_call(layer_kernel, in_specs=[hbm] * 14, out_specs=hbm, out_shap...]
where the time goes in v4:
time: 123 us
  Pallas kernels  120 us (98%)
  local copies, waits for them, and re-layouts  2.3 us (2%)
    pallas_call x1, Pallas kernels, half_slice(): pl.pallas_call(layer_kernel, in_specs=[hbm] * 14, out_specs=hbm, out_shap...  120 us

profile of v4, /device:TPU:0, one launch (start us, length us, event | category | flops | bytes accessed | tf_op | source)
XLA Modules:
  0.0 122.6 jit_solution(5838182346300180029)
XLA Ops:
  0.0 120.2 %shard_map.136 = bf16[256,2048]{1,0:T(8,128)(2,1)} custom-call(bf16[1024,256]{1,0:T(8,128)(2,1)} %outer_hbm.1, bf16[1024,256]{1,0:T(8,128)(2,1)} %inner_hbm.1, bf16[1024,256]{1,0:T(8,128)(2,1)} %input_hbm.1, bf16[3,256]{1,0:T(4,128)(2,1)} %taps_hbm.1, bf16[256,2048]{1,0:T(8,128)(2,1)} %weight_hbm.1, bf16[256,2048]{1,0:T(8,128)(2,1)} %residual_hbm.1, ...), custom_call_target="tpu_custom_call" | custom-call | tf_op jit(solution)/shard_map/pallas_call | solution.py:431
  120.3 2.3 %copy.16 = bf16[256,2048]{1,0:T(8,128)(2,1)} copy(bf16[256,2048]{1,0:T(8,128)(2,1)} %shard_map.136) | data formatting | bytes 2097152

commit v5 on v4

--- a/solution.py
+++ b/solution.py
@@ -25,7 +25,7 @@
 GAIN_ROWS = 16
 HALO_ROWS = 16
 PARTS = 4
-COPIES = 67
+COPIES = 69
 
 
 def layer_kernel(
@@ -161,8 +161,9 @@
         pair = pl.ds((number // 2) * 2 * deep, 2 * deep)
         if number in (1, 3):
             sends.append(send(both.at[1, cut, pair], both.at[1, target, pair], core))
-        if number == 7:
-            sends.append(send(down.at[1, cut], down.at[1, target], core))
+        if number in (5, 7):
+            some = pl.ds((number - 5) * wide, 2 * wide)
+            sends.append(send(down.at[1, cut, some], down.at[1, target, some], core))
 
     def z_arrived(number):
         z_part[number].wait_recv()
@@ -306,15 +307,14 @@
             columns[slot, pair_at[part], piece:] = there[take]
     z_arrived(6)
     z_arrived(7)
-    line_arrived(3)
-    for number in range(4, 8):
+    for number in range(3, 7):
         line_arrived(number)
     for copy in fetched[3:]:
         copy.wait()
-    for copy in z_core + z_both:
+    for copy in z_core[:2] + z_both[:2]:
         copy.wait_recv()
 
-    def expert_sum(unit, store):
+    def expert_hidden(unit):
         rows_in = tokens[unit]
         for slot in range(slots):
             scale_in = columns[slot, unit]
@@ -323,6 +323,8 @@
                 gated = jax.nn.silu(act[:, :units]) * act[:, units:]
                 start = (slot * cuts + cut) * units
                 hidden_sc[:, start : start + units] = (scale_in * gated).astype(jnp.bfloat16)
+
+    def expert_down(store):
         hidden = hidden_sc[...]
         step = width // 4
         for tile in range(4):
@@ -330,6 +332,10 @@
             matrix = down[:, :, :, tile * step : (tile + 1) * step].reshape(slots * cuts * units, step)
             store(columns_at, jnp.dot(hidden, matrix, preferred_element_type=jnp.float32))
 
+    def expert_sum(unit, store):
+        expert_hidden(unit)
+        expert_down(store)
+
     pairs, lines, returned = [], [], []
 
     def pair_step(part):
@@ -339,7 +345,14 @@
             hold[part, :, columns_at] = value[:piece]
             pair_out[part, :, columns_at] = value[piece:].astype(jnp.bfloat16)
 
-        expert_sum(pair_at[part], store)
+        if part == 0:
+            expert_hidden(pair_at[0])
+            line_arrived(7)
+            for copy in z_core[2:] + z_both[2:]:
+                copy.wait_recv()
+            expert_down(store)
+        else:
+            expert_sum(pair_at[part], store)
         pairs.append(send(pair_out.at[part], pair_in.at[part], x_peer))
 
     def return_step(part):
@@ -376,10 +389,10 @@
     pair_step(2)
     own_step(1)
     pair_step(3)
+    line_step(0)
     return_step(2)
-    line_step(0)
+    line_step(1)
     return_step(3)
-    line_step(1)
     late = pairs + lines + returned + halos
     only(jnp.logical_not(last_block), lambda copy: copy.wait_send(), *halos)
     for copy in started:

time: 123 us -> 122 us (level)
  no operation moved by 1% of the time
where the time goes in v5:
time: 122 us
  Pallas kernels  119 us (98%)
  local copies, waits for them, and re-layouts  2.3 us (2%)
    pallas_call x1, Pallas kernels, half_slice(): pl.pallas_call(layer_kernel, in_specs=[hbm] * 14, out_specs=hbm, out_shap...  119 us

profile of v5, /device:TPU:0, one launch (start us, length us, event | category | flops | bytes accessed | tf_op | source)
XLA Modules:
  0.0 121.7 jit_solution(234853290977804861)
XLA Ops:
  0.0 119.4 %shard_map.136 = bf16[256,2048]{1,0:T(8,128)(2,1)} custom-call(bf16[1024,256]{1,0:T(8,128)(2,1)} %outer_hbm.1, bf16[1024,256]{1,0:T(8,128)(2,1)} %inner_hbm.1, bf16[1024,256]{1,0:T(8,128)(2,1)} %input_hbm.1, bf16[3,256]{1,0:T(4,128)(2,1)} %taps_hbm.1, bf16[256,2048]{1,0:T(8,128)(2,1)} %weight_hbm.1, bf16[256,2048]{1,0:T(8,128)(2,1)} %residual_hbm.1, ...), custom_call_target="tpu_custom_call" | custom-call | tf_op jit(solution)/shard_map/pallas_call | solution.py:444
  119.4 2.3 %copy.16 = bf16[256,2048]{1,0:T(8,128)(2,1)} copy(bf16[256,2048]{1,0:T(8,128)(2,1)} %shard_map.136) | data formatting | bytes 2097152
